TPU v7x, 32 devices: a whole 2x2x4 slice. The times are simulated.
32 devices in a mesh: ep: 16 (over z, y, x), tp: 2 (over core).
Axes of the slice: x: 2, y: 2, z: 4, core: 2. Of those that a mesh axis runs over, the one named last changes fastest.
Arguments:
- tokens: bfloat16 [384, 2048], P('ep'), may hold values from -6 to 6
- attn_gain: float32 [2048], replicated, may hold values from 0.1 to 1.9
- w_query: bfloat16 [2048, 1024], P(None, 'tp'), may hold values from -0.125 to 0.125
- w_key: bfloat16 [2048, 1024], P(None, 'tp'), may hold values from -0.125 to 0.125
- w_value: bfloat16 [2048, 1024], P(None, 'tp'), may hold values from -0.125 to 0.125
- w_zgate: bfloat16 [2048, 1024], P(None, 'tp'), may hold values from -0.125 to 0.125
- w_decay: bfloat16 [2048, 8], P(None, 'tp'), may hold values from -0.125 to 0.125
- w_beta: bfloat16 [2048, 8], P(None, 'tp'), may hold values from -0.125 to 0.125
- decay_rate: float32 [8], P('tp'), may hold values from 0.05 to 2
- decay_bias: float32 [8], P('tp'), may hold values from -3 to 3
- state: float32 [384, 8, 128, 128], P('ep', 'tp'), may hold values from -2 to 2
- out_gain: float32 [128], replicated, may hold values from 0.1 to 1.9
- w_out: bfloat16 [1024, 2048], P('tp'), may hold values from -0.1875 to 0.1875
- ffn_gain: float32 [2048], replicated, may hold values from 0.1 to 1.9
- expert_gate: bfloat16 [16, 2048, 512], P('ep', None, 'tp'), may hold values from -0.125 to 0.125
- expert_up: bfloat16 [16, 2048, 512], P('ep', None, 'tp'), may hold values from -0.125 to 0.125
- expert_down: bfloat16 [16, 512, 2048], P('ep', 'tp'), may hold values from -0.25 to 0.25
- routes: int32 [384, 2], P('ep'), may hold values from 0 to 15, all different within a row; in each aligned block of 24 rows (0 to 23, 24 to 47, ...) at most 6 rows name the same one
- route_weight: float32 [384, 2], P('ep'), may hold values from 0.2 to 1
Outputs:
- layer_out: bfloat16 [384, 2048], P('ep', 'tp')
- new_state: float32 [384, 8, 128, 128], P('ep', 'tp')
Inputs may be any that keep to these rules, and one draw needn't show every extreme that they name: `routes`: the 2 entries of a row differ. Among the rows of one index of ep (aligned blocks of 24 rows) no expert is named more than 6 times, a bound that some block reaches.
All inputs are finite; a program needn't handle non-finite values.
Results may differ from a plain program's by a relative error of at most 0.014.
Values may be sent and summed in bfloat16 or wider, within the bound.
No kernel may reach another device: no remote copies, remote signals or barrier semaphores. Data moves between devices by JAX's collectives and lax.ppermute only.
A program may use at most 128 MiB of HBM per device.

v0:
```python
import jax
import jax.numpy as jnp
from jax import lax
from jax.sharding import PartitionSpec as P

EPS = 1e-06


def rms_scale(rows, gain):
    return rows * lax.rsqrt(jnp.mean(rows * rows, axis=-1, keepdims=True) + EPS) * gain


def unit_rows(rows):
    return rows * lax.rsqrt(jnp.sum(rows * rows, axis=-1, keepdims=True) + EPS)


def per_device(
    tokens,
    attn_gain,
    w_query,
    w_key,
    w_value,
    w_zgate,
    w_decay,
    w_beta,
    decay_rate,
    decay_bias,
    state,
    out_gain,
    w_out,
    ffn_gain,
    expert_gate,
    expert_up,
    expert_down,
    routes,
    route_weight,
):
    seqs, width = tokens.shape
    heads = state.shape[1]
    head_dim = state.shape[2]
    top = routes.shape[1]
    resid_in = tokens.astype(jnp.float32)
    normed = rms_scale(resid_in, attn_gain).astype(jnp.bfloat16)

    def project(weight):
        return jnp.dot(normed, weight, preferred_element_type=jnp.float32).astype(jnp.bfloat16)

    def heads_of(raw):
        return raw.reshape(seqs, heads, head_dim).astype(jnp.float32)

    query = unit_rows(jax.nn.silu(heads_of(project(w_query)))) * head_dim ** (-0.5)
    key = unit_rows(jax.nn.silu(heads_of(project(w_key))))
    value = jax.nn.silu(heads_of(project(w_value)))
    zmul = jax.nn.silu(heads_of(project(w_zgate)))
    fade = jnp.exp(-decay_rate * jax.nn.softplus(project(w_decay).astype(jnp.float32) + decay_bias))
    beta = jax.nn.sigmoid(project(w_beta).astype(jnp.float32))
    predicted = jnp.einsum("shkv,shk->shv", state, key, precision=lax.Precision.HIGHEST)
    written = beta[..., None] * (value - fade[..., None] * predicted)
    new_state = fade[..., None, None] * state + key[..., :, None] * written[..., None, :]
    read = jnp.einsum("shkv,shk->shv", new_state, query, precision=lax.Precision.HIGHEST)
    heads_out = (
        (rms_scale(read, out_gain) * zmul).astype(jnp.bfloat16).reshape(seqs, heads * head_dim)
    )
    partial_value = jnp.dot(heads_out, w_out, preferred_element_type=jnp.float32)
    mixed = lax.psum(partial_value.astype(jnp.bfloat16), "tp").astype(jnp.float32)
    resid = resid_in + mixed
    moe_in = rms_scale(resid, ffn_gain).astype(jnp.bfloat16)
    experts = lax.axis_size("ep")
    cap = max(2, 2 * seqs * top // experts)
    flat_routes = routes.reshape(-1)
    onehot = (flat_routes[:, None] == jnp.arange(experts, dtype=jnp.int32)[None, :]).astype(
        jnp.int32
    )
    before = jnp.cumsum(onehot, axis=0) - onehot
    slot = jnp.sum(before * onehot, axis=1)
    place = flat_routes * cap + slot
    pick = (place[:, None] == jnp.arange(experts * cap, dtype=jnp.int32)[None, :]).astype(
        jnp.bfloat16
    )
    columns = width // lax.axis_size("tp")
    own_part = lax.dynamic_slice_in_dim(moe_in, lax.axis_index("tp") * columns, columns, 1)
    spread = jnp.repeat(own_part, top, axis=0)
    outgoing = jnp.dot(pick.T, spread, preferred_element_type=jnp.float32).astype(jnp.bfloat16)
    outgoing = outgoing.reshape(experts, 1, cap, columns)
    arrived = lax.all_gather(
        lax.all_to_all(outgoing, "ep", split_axis=0, concat_axis=1, tiled=True),
        "tp",
        axis=3,
        tiled=True,
    )
    flat_rows = arrived.reshape(-1, arrived.shape[-1])
    gate = jnp.dot(flat_rows, expert_gate[0], preferred_element_type=jnp.float32)
    up = jnp.dot(flat_rows, expert_up[0], preferred_element_type=jnp.float32)
    hidden = (jax.nn.silu(gate) * up).astype(jnp.bfloat16)
    term = jnp.dot(hidden, expert_down[0], preferred_element_type=jnp.float32)
    terms = term.reshape(arrived.shape[:-1] + (term.shape[-1],))
    summed = lax.psum_scatter(terms.astype(jnp.bfloat16), "tp", scatter_dimension=3, tiled=True)
    returned = lax.all_to_all(summed, "ep", split_axis=1, concat_axis=0, tiled=True)
    returned = returned.reshape(experts * cap, columns)
    per_route = jnp.dot(pick, returned, preferred_element_type=jnp.float32).reshape(
        seqs, top, columns
    )
    combined = jnp.sum(per_route * route_weight[..., None], axis=1)
    own_resid = lax.dynamic_slice_in_dim(resid, lax.axis_index("tp") * columns, columns, 1)
    layer_out = (own_resid + combined).astype(jnp.bfloat16)
    return (layer_out, new_state)


def solution(mesh):
    in_specs = (
        P("ep", None),
        P(),
        P(None, "tp"),
        P(None, "tp"),
        P(None, "tp"),
        P(None, "tp"),
        P(None, "tp"),
        P(None, "tp"),
        P("tp"),
        P("tp"),
        P("ep", "tp", None, None),
        P(),
        P("tp", None),
        P(),
        P("ep", None, "tp"),
        P("ep", None, "tp"),
        P("ep", "tp", None),
        P("ep", None),
        P("ep", None),
    )
    out_specs = (P("ep", "tp"), P("ep", "tp", None, None))
    return jax.shard_map(
        per_device, mesh=mesh, in_specs=in_specs, out_specs=out_specs, check_vma=False
    )
```

profile of v0, /device:TPU:0, one launch (start us, length us, event | category | flops | bytes accessed | tf_op | source)
XLA Modules:
  0.0 115.3 jit_solution(10898759450930380615)
XLA Ops:
  7.3 1.2 %fusion.18 = f32[24]{0:T(128)S(1)} fusion(bf16[24,2048]{1,0:T(8,128)(2,1)} %param.19), kind=kLoop, calls=%fused_computation.33 | loop fusion | flops 147432 | bytes 98400 | tf_op jit(solution)/shard_map/reduce_sum | solution.py:10
  8.5 2.1 %fusion.6 = f32[24,512]{1,0:T(8,128)S(1)} fusion(bf16[2048,512]{1,0:T(8,128)(2,1)} %param.22, bf16[24,2048]{1,0:T(8,128)(2,1)} %param.19, f32[2048]{0:T(1024)} %param.20, f32[24]{0:T(128)S(1)} %add_rsqrt_fusion.4), kind=kOutput, calls=%fused_computation.16 | convolution fusion | flops 50552832 | bytes 2252896 | tf_op jit(solution)/shard_map/dot_general | solution.py:46
  10.6 0.1 multiply_reduce_fusion.3
  10.9 0.2 fusion.34
  11.2 2.0 %fusion.5 = f32[24,512]{1,0:T(8,128)S(1)} fusion(bf16[2048,512]{1,0:T(8,128)(2,1)} %param.23, bf16[24,2048]{1,0:T(8,128)(2,1)S(1)} %copy-done.2, f32[2048]{0:T(1024)S(1)} %copy-done.5, f32[24]{0:T(128)S(1)} %add_rsqrt_fusion.4), kind=kOutput, calls=%fused_computation.14 | convolution fusion | flops 50552832 | bytes 2252896 | tf_op jit(solution)/shard_map/dot_general | solution.py:46
  13.3 0.2 fusion.13
  13.6 8.1 %fusion.41 = f32[24,4,1,128]{3,2,1,0:T(1,128)S(1)} fusion(f32[24,4,128,1]{2,3,1,0:T(1,128)S(1)} %bitcast.48, f32[24,4,128,128]{3,2,1,0:T(8,128)} %param.29), kind=kOutput, calls=%fused_computation.73 | convolution fusion | flops 18874368 | bytes 6389760 | tf_op jit(solution)/shard_map/shkv,shk->shv/dot_general | solution.py:57
  21.7 0.1 fusion.24
  21.8 3.9 %multiply_add_fusion = f32[24,4,128,128]{3,2,1,0:T(8,128)} fusion(f32[24,4,128,128]{3,2,1,0:T(8,128)S(1)} %copy-done.1, f32[24,4,128]{2,1,0:T(4,128)S(1)} %fusion.24, f32[24,4,128]{2,1,0:T(4,128)S(1)} %broadcast_multiply_fusion, f32[24,4]{1,0:T(8,128)S(1)} %copy.48), kind=kLoop, calls=%fused_computation | loop fusion | flops 4718592 | bytes 12681600 | tf_op jit(solution)/shard_map/add | solution.py:59
  25.7 0.4 fusion.4
  26.2 0.1 multiply_reduce_fusion.2
  26.4 7.5 %fusion.42 = f32[24,4,1,128]{3,2,1,0:T(1,128)S(1)} fusion(f32[24,4,128,128]{3,2,1,0:T(8,128)} %multiply_add_fusion, f32[24,4,128,1]{2,3,1,0:T(1,128)S(1)} %bitcast.51), kind=kOutput, calls=%fused_computation.74 | convolution fusion | flops 18874368 | bytes 6389760 | tf_op jit(solution)/shard_map/shkv,shk->shv/dot_general | solution.py:60
  33.9 0.1 multiply_reduce_fusion.1
  34.1 0.4 fusion.3
  34.6 0.1 fusion.25
  34.7 1.0 convolution_convert_fusion.1
  36.2 0.2 select_reduce_fusion
  36.4 20.1 %all-reduce.2.cloned.1.call-done = bf16[24,2048]{1,0:T(8,128)(2,1)} async-done(((bf16[24,2048]{1,0:T(8,128)(2,1)}), bf16[24,2048]{1,0:T(8,128)(2,1)}) %all-reduce.2.cloned.1.call-update) | async-done | bytes 98320 | tf_op jit(solution)/shard_map/psum | solution.py:65
  56.5 1.0 multiply_reduce_fusion
  57.7 0.3 convolution_convert_fusion.2
  58.1 16.9 %all_to_all.21 = bf16[16,1,6,1024]{3,2,1,0:T(8,128)(2,1)S(1)} all-to-all(bf16[16,1,6,1024]{3,2,1,0:T(8,128)(2,1)S(1)} %bitcast.47), channel_id=1, replica_groups=mesh['ep'=16,'tp'=2] {'ep'}, dimensions={0} | all-to-all | bytes 393216 | tf_op jit(solution)/shard_map/all_to_all | solution.py:86
  75.0 2.2 %all-gather = bf16[16,1,6,2048]{3,2,1,0:T(8,128)(2,1)S(1)} all-gather(bf16[16,1,6,1024]{3,2,1,0:T(8,128)(2,1)S(1)} %all_to_all.21), channel_id=2, replica_groups=mesh['ep'=16,'tp'=2] {'tp'}, dimensions={3}, use_global_device_ids=true | all-gather | bytes 589824 | tf_op jit(solution)/shard_map/all_gather | solution.py:85
  77.2 0.1 reshape.137
  77.3 1.5 %fusion.16 = f32[96,256]{1,0:T(8,128)S(1)} fusion(bf16[96,2048]{1,0:T(8,128)(2,1)S(1)} %reshape.137, bf16[1,2048,256]{2,1,0:T(8,128)(2,1)} %param.33), kind=kOutput, calls=%fused_computation.28 | convolution fusion | flops 100663296 | bytes 1540096 | tf_op jit(solution)/shard_map/dot_general | solution.py:92
  78.9 1.5 %fusion.2 = bf16[96,256]{1,0:T(8,128)(2,1)S(1)} fusion(bf16[96,2048]{1,0:T(8,128)(2,1)S(1)} %reshape.137, bf16[1,2048,256]{2,1,0:T(8,128)(2,1)} %param.34, f32[96,256]{1,0:T(8,128)S(1)} %fusion.16), kind=kOutput, calls=%fused_computation.8 | convolution fusion | flops 100810752 | bytes 1589248 | tf_op jit(solution)/shard_map/dot_general | solution.py:93
  80.5 2.3 %fusion = bf16[1,16,6,2048]{3,1,2,0:T(8,128)(2,1)} fusion(bf16[1,256,2048]{2,1,0:T(8,128)(2,1)} %param.35, bf16[16,6,256]{2,1,0:T(8,128)(2,1)S(1)} %dot_general.56), kind=kOutput, calls=%fused_computation.2 | convolution fusion | flops 100859904 | bytes 1490944 | tf_op jit(solution)/shard_map/dot_general | solution.py:95
  82.8 5.9 %reduce-scatter.2.cloned.1.call-done = bf16[1,16,6,1024]{3,1,2,0:T(8,128)(2,1)} async-done(((bf16[1,16,6,2048]{3,1,2,0:T(8,128)(2,1)}), bf16[1,16,6,1024]{3,1,2,0:T(8,128)(2,1)}) %reduce-scatter.2.cloned.1.call-update) | async-done | bytes 196624 | tf_op jit(solution)/shard_map/reduce_scatter | solution.py:97
  88.6 1.7 %copy.55 = bf16[1,16,6,1024]{3,2,0,1:T(8,128)(2,1)} copy(bf16[1,16,6,1024]{3,1,2,0:T(8,128)(2,1)} %reduce-scatter.2.cloned.1.call-done) | data formatting | bytes 393216 | tf_op jit(solution)/shard_map/reduce_scatter | solution.py:97
  90.4 6.7 %all-to-all-start.1 = ((bf16[1,16,6,1024]{3,2,0,1:T(8,128)(2,1)}), bf16[1,16,6,1024]{3,2,0,1:T(8,128)(2,1)S(1)}, u32[]{:S(2)}, u32[]{:S(2)}) async-start(bf16[1,16,6,1024]{3,2,0,1:T(8,128)(2,1)} %copy.55), calls=%async_computation.2 | async-start | bytes 524288 | tf_op jit(solution)/shard_map/all_to_all | solution.py:98
  97.3 10.2 %all-to-all-done.1 = bf16[1,16,6,1024]{3,2,0,1:T(8,128)(2,1)S(1)} async-done(((bf16[1,16,6,1024]{3,2,0,1:T(8,128)(2,1)}), bf16[1,16,6,1024]{3,2,0,1:T(8,128)(2,1)S(1)}, u32[]{:S(2)}, u32[]{:S(2)}) %all-to-all-start.1) | async-done | bytes 196640 | tf_op jit(solution)/shard_map/all_to_all | solution.py:98
  107.6 0.2 fusion.1
  107.8 0.6 add_convert_fusion
  (61 shorter events, 1.6 us)
Async XLA Ops:
  7.2 27.5 %copy-start = (bf16[512,2048]{1,0:T(8,128)(2,1)S(1)}, bf16[512,2048]{1,0:T(8,128)(2,1)}, u32[]{:S(2)}) copy-start(bf16[512,2048]{1,0:T(8,128)(2,1)} %param.31) | copy-start | bytes 6291460
  7.2 3.7 %copy-start.2 = (bf16[24,2048]{1,0:T(8,128)(2,1)S(1)}, bf16[24,2048]{1,0:T(8,128)(2,1)}, u32[]{:S(2)}) copy-start(bf16[24,2048]{1,0:T(8,128)(2,1)} %param.19) | copy-start | bytes 294916
  7.2 3.7 %copy-start.5 = (f32[2048]{0:T(1024)S(1)}, f32[2048]{0:T(1024)}, u32[]{:S(2)}) copy-start(f32[2048]{0:T(1024)} %param.20) | copy-start | bytes 24580
  7.2 3.6 %copy-start.12 = (f32[4]{0:T(128)S(1)}, f32[4]{0:T(128)}, u32[]{:S(2)}) copy-start(f32[4]{0:T(128)} %param.27) | copy-start | bytes 52
  7.2 3.7 %copy-start.10 = (bf16[2048,4]{0,1:T(4,128)(2,1)S(1)}, bf16[2048,4]{0,1:T(4,128)(2,1)}, u32[]{:S(2)}) copy-start(bf16[2048,4]{0,1:T(4,128)(2,1)} %param.25) | copy-start | bytes 49156
  7.2 3.7 %copy-start.13 = (f32[4]{0:T(128)S(1)}, f32[4]{0:T(128)}, u32[]{:S(2)}) copy-start(f32[4]{0:T(128)} %param.28) | copy-start | bytes 52
  7.2 49.2 %all-reduce.2.cloned.1.call-start = ((), (), s32[]{:S(2)}) async-start(), calls=%async_computation.3 | async-start | bytes 196608 | tf_op jit(solution)/shard_map/psum | solution.py:65
  8.4 4.8 %copy-start.11 = (bf16[2048,4]{0,1:T(4,128)(2,1)S(1)}, bf16[2048,4]{0,1:T(4,128)(2,1)}, u32[]{:S(2)}) copy-start(bf16[2048,4]{0,1:T(4,128)(2,1)} %param.26) | copy-start | bytes 49156
  13.6 8.2 %copy-start.1 = (f32[24,4,128,128]{3,2,1,0:T(8,128)S(1)}, f32[24,4,128,128]{3,2,1,0:T(8,128)}, u32[]{:S(2)}) copy-start(f32[24,4,128,128]{3,2,1,0:T(8,128)} %param.29) | copy-start | bytes 18874372
  21.8 3.9 %copy-start.3 = (bf16[2048,512]{1,0:T(8,128)(2,1)S(1)}, bf16[2048,512]{1,0:T(8,128)(2,1)}, u32[]{:S(2)}) copy-start(bf16[2048,512]{1,0:T(8,128)(2,1)} %param.21) | copy-start | bytes 6291460
  26.4 7.7 %copy-start.4 = (bf16[2048,512]{1,0:T(8,128)(2,1)S(1)}, bf16[2048,512]{1,0:T(8,128)(2,1)}, u32[]{:S(2)}) copy-start(bf16[2048,512]{1,0:T(8,128)(2,1)} %param.24) | copy-start | bytes 6291460
  33.9 0.7 copy-start.9
  34.1 1.7 %copy-start.6 = (s32[24,2]{0,1:T(2,128)S(1)}, s32[24,2]{0,1:T(2,128)}, u32[]{:S(2)}) copy-start(s32[24,2]{0,1:T(2,128)} %param.36) | copy-start | bytes 580
  34.1 2.3 %copy-start.7 = (f32[2048]{0:T(1024)S(1)}, f32[2048]{0:T(1024)}, u32[]{:S(2)}) copy-start(f32[2048]{0:T(1024)} %param.32) | copy-start | bytes 24580
  35.8 52.9 %reduce-scatter.2.cloned.1.call-start = ((), (), s32[]{:S(2)}) async-start(), calls=%async_computation.4 | async-start | bytes 589824 | tf_op jit(solution)/shard_map/reduce_scatter | solution.py:97
  80.4 27.2 %copy-start.8 = (f32[24,2]{0,1:T(2,128)S(1)}, f32[24,2]{0,1:T(2,128)}, u32[]{:S(2)}) copy-start(f32[24,2]{0,1:T(2,128)} %param.37) | copy-start | bytes 580
  90.4 17.1 %all-to-all-start.1 = ((bf16[1,16,6,1024]{3,2,0,1:T(8,128)(2,1)}), bf16[1,16,6,1024]{3,2,0,1:T(8,128)(2,1)S(1)}, u32[]{:S(2)}, u32[]{:S(2)}) async-start(bf16[1,16,6,1024]{3,2,0,1:T(8,128)(2,1)} %copy.55), calls=%async_computation.2 | async-start | bytes 524288 | tf_op jit(solution)/shard_map/all_to_all | solution.py:98
Sparse Core Ops, SparseCore 0:
  35.9 20.5 all-reduce.1
  82.9 5.7 reduce-scatter.1
where the time goes:
time: 116 us; the launch traced here: 115 us
  waiting for transfers between devices  36.2 us (31%)
  matrix products  28 us (24%)
  blocking collectives  19.1 us (16%)
  between operations  14.4 us (12%)
  other arithmetic  7.91 us (7%)
  starting transfers between devices  6.81 us (6%)
  local copies, waits for them, and re-layouts  2.86 us (2%)
    psum x1, waiting for transfers between devices, per_device(): lax.psum(partial_value.astype(jnp.bfloat16), 'tp').astype(jnp.float32)  20.1 us
    all_to_all x1, blocking collectives, per_device(): lax.all_to_all(outgoing, 'ep', split_axis=0, concat_axis=1, tiled=True)  16.9 us
    all_to_all x1, waiting for transfers between devices, per_device(): lax.all_to_all(summed, 'ep', split_axis=1, concat_axis=0, tiled=True)  10.2 us
    dot_general x1, matrix products, per_device(): jnp.einsum('shkv,shk->shv', state, key, precision=lax.Precision.HIGHEST)  8.09 us
    dot_general x1, matrix products, per_device(): jnp.einsum('shkv,shk->shv', new_state, query, precision=lax.Precision.HIG...  7.54 us
    all_to_all x1, starting transfers between devices, per_device(): lax.all_to_all(summed, 'ep', split_axis=1, concat_axis=0, tiled=True)  6.73 us
    reduce_scatter x1, waiting for transfers between devices, per_device(): lax.psum_scatter(terms.astype(jnp.bfloat16), 'tp', scatter_dimension=3, t...  5.89 us
    dot_general x6, matrix products, project(): jnp.dot(normed, weight, preferred_element_type=jnp.float32)  5.45 us
  transfers between devices with their start and end apart: 3, of which 3 were waited for; matrix products, arithmetic and copies ran while one was open for 1% of the time, Pallas kernels for 0%

commit v1 on v0

v1 whole, which is shorter than its diff:
```python
import jax
import jax.numpy as jnp
from jax import lax
from jax.experimental import pallas as pl
from jax.experimental.pallas import tpu as pltpu
from jax.sharding import PartitionSpec as P

EPS = 1e-06
BF16 = jnp.bfloat16
F32 = jnp.float32


def rms_scale(rows, gain):
    return rows * lax.rsqrt(jnp.mean(rows * rows, axis=-1, keepdims=True) + EPS) * gain


def unit_rows(rows):
    return rows * lax.rsqrt(jnp.sum(rows * rows, axis=-1, keepdims=True) + EPS)


def silu(x):
    return x * jax.nn.sigmoid(x)


def chunk_of(seqs):
    return next(c for c in (4, 3, 2, 1) if seqs % c == 0)


def mixer_kernel(
    tokens_ref, again_ref, wa_ref, wb_ref, rate_ref, bias_ref, ogain_ref,
    wq_hbm, wk_hbm, wv_hbm, wz_hbm, state_hbm, wo_hbm,
    part_ref, new_hbm,
    wq, wk, wv, wz, wo, st, kq, vb, fb, bb, rd, zb, wsem, isem, osem,
):
    seqs, heads, dim, _ = st.shape
    chunk = chunk_of(seqs)
    chunks = seqs // chunk

    def weight(i):
        src, dst = ((wk_hbm, wk), (wq_hbm, wq), (wv_hbm, wv), (wz_hbm, wz), (wo_hbm, wo))[i]
        return pltpu.make_async_copy(src, dst, wsem.at[i])

    def rows_of(c):
        return pl.ds(c * chunk, chunk)

    def state_in(c):
        return pltpu.make_async_copy(state_hbm.at[rows_of(c)], st.at[rows_of(c)], isem.at[c])

    def state_out(c):
        return pltpu.make_async_copy(st.at[rows_of(c)], new_hbm.at[rows_of(c)], osem.at[c])

    for i in range(3):
        weight(i).start()
    for c in range(chunks):
        state_in(c).start()
    weight(3).start()
    weight(4).start()

    normed = rms_scale(tokens_ref[...].astype(F32), again_ref[...]).astype(BF16)

    def narrow(ref):
        raw = lax.dot_general(normed, ref[...], (((1,), (1,)), ((), ())), preferred_element_type=F32)
        return raw.astype(BF16).astype(F32)

    raw_a = narrow(wa_ref) + bias_ref[...]
    softplus = jnp.maximum(raw_a, 0.0) + jnp.log1p(jnp.exp(-jnp.abs(raw_a)))
    fade = jnp.exp(-rate_ref[...] * softplus)
    beta = jax.nn.sigmoid(narrow(wb_ref))
    for h in range(heads):
        fb[:, h, :] = jnp.broadcast_to(fade[:, h : h + 1], (seqs, dim))
        bb[:, h, :] = jnp.broadcast_to(beta[:, h : h + 1], (seqs, dim))

    def project(ref):
        raw = jnp.dot(normed, ref[...], preferred_element_type=F32)
        return silu(raw.astype(BF16).astype(F32))

    def head(x, h):
        return x[:, h * dim : (h + 1) * dim]

    weight(0).wait()
    key = project(wk)
    for h in range(heads):
        kq[:, h, :] = unit_rows(head(key, h))
    weight(1).wait()
    query = project(wq)
    for h in range(heads):
        kq[:, heads + h, :] = unit_rows(head(query, h)) * dim ** (-0.5)
    weight(2).wait()
    value = project(wv)
    for h in range(heads):
        vb[:, h, :] = head(value, h)

    def body(c, carry):
        state_in(c).wait()
        for i in range(chunk):
            s = c * chunk + i
            turned = kq[s].T
            fades, betas, values = fb[s], bb[s], vb[s]
            for h in range(heads):
                old = st[s, h] * fades[h : h + 1]
                kcol = turned[:, h : h + 1]
                qcol = turned[:, heads + h : heads + h + 1]
                predicted = jnp.sum(old * kcol, axis=0, keepdims=True)
                written = betas[h : h + 1] * (values[h : h + 1] - predicted)
                new = old + kcol * written
                st[s, h] = new
                rd[s, pl.ds(h, 1), :] = jnp.sum(new * qcol, axis=0, keepdims=True)
        state_out(c).start()
        return carry

    lax.fori_loop(0, chunks, body, 0)
    weight(3).wait()
    zb[...] = project(wz)
    outs = []
    for h in range(heads):
        outs.append((rms_scale(rd[:, h, :], ogain_ref[...]) * head(zb[...], h)).astype(BF16))
    weight(4).wait()
    part_ref[...] = jnp.dot(
        jnp.concatenate(outs, axis=1), wo[...], preferred_element_type=F32
    ).astype(BF16)
    for c in range(chunks):
        state_out(c).wait()


def mixer(tokens, attn_gain, wq, wk, wv, wz, wa, wb, rate, bias, state, out_gain, wo):
    seqs, width = tokens.shape
    heads, dim = state.shape[1:3]
    chunks = seqs // chunk_of(seqs)
    vm = pl.BlockSpec(memory_space=pltpu.VMEM)
    hbm = pl.BlockSpec(memory_space=pl.ANY)
    flat = heads * dim
    return pl.pallas_call(
        mixer_kernel,
        out_shape=(
            jax.ShapeDtypeStruct((seqs, wo.shape[1]), BF16),
            jax.ShapeDtypeStruct(state.shape, F32),
        ),
        in_specs=[vm] * 7 + [hbm] * 6,
        out_specs=(vm, hbm),
        scratch_shapes=[pltpu.VMEM((width, flat), BF16)] * 4
        + [pltpu.VMEM(wo.shape, BF16), pltpu.VMEM(state.shape, F32)]
        + [pltpu.VMEM((seqs, 2 * heads, dim), F32)]
        + [pltpu.VMEM((seqs, heads, dim), F32)] * 4
        + [pltpu.VMEM((seqs, flat), F32)]
        + [
            pltpu.SemaphoreType.DMA((5,)),
            pltpu.SemaphoreType.DMA((chunks,)),
            pltpu.SemaphoreType.DMA((chunks,)),
        ],
        compiler_params=pltpu.CompilerParams(vmem_limit_bytes=48 << 20),
        name="mixer",
    )(
        tokens, attn_gain[None], wa.T, wb.T, rate[None], bias[None], out_gain[None],
        wq, wk, wv, wz, state, wo,
    )


def dispatch_kernel(side_ref, tokens_ref, part_ref, other_ref, gain_ref, pick_ref, out_ref, res_ref, buf):
    mixed = part_ref[...].astype(F32) + other_ref[...].astype(F32)
    buf[...] = tokens_ref[...].astype(F32) + mixed
    resid = buf[...]
    cols = out_ref.shape[1]
    own = pl.ds(pl.multiple_of(side_ref[0] * cols, cols), cols)
    scale = lax.rsqrt(jnp.mean(resid * resid, axis=-1, keepdims=True) + EPS)
    own_resid = buf[:, own]
    moe_in = (own_resid * scale * gain_ref[:, own]).astype(BF16)
    out_ref[...] = jnp.dot(pick_ref[...], moe_in, preferred_element_type=F32).astype(BF16)
    res_ref[...] = own_resid


def dispatch(side, tokens, part, other, gain, pick, cols):
    seqs, width = tokens.shape
    vm = pl.BlockSpec(memory_space=pltpu.VMEM)
    return pl.pallas_call(
        dispatch_kernel,
        out_shape=(
            jax.ShapeDtypeStruct((pick.shape[0], cols), BF16),
            jax.ShapeDtypeStruct((seqs, cols), F32),
        ),
        in_specs=[pl.BlockSpec(memory_space=pltpu.SMEM)] + [vm] * 5,
        out_specs=(vm, vm),
        scratch_shapes=[pltpu.VMEM((seqs, width), F32)],
        name="dispatch",
    )(side, tokens, part, other, gain[None], pick)


def expert_kernel(side_ref, own_ref, oth_ref, wg_hbm, wu_hbm, wd_hbm, mine_ref, send_ref, wg, wu, wd, sem):
    copies = [
        pltpu.make_async_copy(src.at[0], dst, sem.at[i])
        for i, (src, dst) in enumerate(((wg_hbm, wg), (wu_hbm, wu), (wd_hbm, wd)))
    ]
    for copy in copies:
        copy.start()
    cols = own_ref.shape[1]
    side = side_ref[0]
    own = pl.ds(pl.multiple_of(side * cols, cols), cols)
    oth = pl.ds(pl.multiple_of((1 - side) * cols, cols), cols)

    def project(ref):
        return jnp.dot(own_ref[...], ref[own, :], preferred_element_type=F32) + jnp.dot(
            oth_ref[...], ref[oth, :], preferred_element_type=F32
        )

    copies[0].wait()
    gate = silu(project(wg))
    copies[1].wait()
    hidden = (gate * project(wu)).astype(BF16)
    copies[2].wait()
    send_ref[...] = jnp.dot(hidden, wd[:, oth], preferred_element_type=F32).astype(BF16)
    mine_ref[...] = jnp.dot(hidden, wd[:, own], preferred_element_type=F32).astype(BF16)


def expert(side, own, oth, wg, wu, wd):
    vm = pl.BlockSpec(memory_space=pltpu.VMEM)
    hbm = pl.BlockSpec(memory_space=pl.ANY)
    half = jax.ShapeDtypeStruct(own.shape, BF16)
    return pl.pallas_call(
        expert_kernel,
        out_shape=(half, half),
        in_specs=[pl.BlockSpec(memory_space=pltpu.SMEM), vm, vm, hbm, hbm, hbm],
        out_specs=(vm, vm),
        scratch_shapes=[pltpu.VMEM(w.shape[1:], BF16) for w in (wg, wu, wd)]
        + [pltpu.SemaphoreType.DMA((3,))],
        name="expert",
    )(side, own, oth, wg, wu, wd)


def per_device(
    tokens,
    attn_gain,
    w_query,
    w_key,
    w_value,
    w_zgate,
    w_decay,
    w_beta,
    decay_rate,
    decay_bias,
    state,
    out_gain,
    w_out,
    ffn_gain,
    expert_gate,
    expert_up,
    expert_down,
    routes,
    route_weight,
):
    seqs, width = tokens.shape
    top = routes.shape[1]
    swap = [(0, 1), (1, 0)]
    experts = lax.axis_size("ep")
    cap = max(2, 2 * seqs * top // experts)
    columns = width // lax.axis_size("tp")
    side = lax.axis_index("tp").astype(jnp.int32).reshape(1)
    partial_value, new_state = mixer(
        tokens, attn_gain, w_query, w_key, w_value, w_zgate, w_decay, w_beta,
        decay_rate, decay_bias, state, out_gain, w_out,
    )
    other = lax.ppermute(partial_value, "tp", swap)

    flat_routes = routes.reshape(-1)
    onehot = (flat_routes[:, None] == jnp.arange(experts, dtype=jnp.int32)[None, :]).astype(jnp.int32)
    before = jnp.cumsum(onehot, axis=0) - onehot
    slot = jnp.sum(before * onehot, axis=1)
    place = flat_routes * cap + slot
    slots = jnp.arange(experts * cap, dtype=jnp.int32)
    pick = (place[:, None] == slots[None, :]).astype(BF16)
    taken = jnp.any(place.reshape(1, seqs, top) == slots[:, None, None], axis=2).astype(BF16)

    outgoing, own_resid = dispatch(side, tokens, partial_value, other, ffn_gain, taken, columns)
    outgoing = outgoing.reshape(experts, cap, columns)
    arrived = lax.all_to_all(outgoing, "ep", split_axis=0, concat_axis=0, tiled=True)
    rows = arrived.reshape(experts * cap, columns)
    mine, send = expert(side, rows, lax.ppermute(rows, "tp", swap), expert_gate, expert_up, expert_down)
    summed = (mine.astype(F32) + lax.ppermute(send, "tp", swap).astype(F32)).astype(BF16)
    summed = summed.reshape(experts, cap, columns)
    returned = lax.all_to_all(summed, "ep", split_axis=0, concat_axis=0, tiled=True)
    returned = returned.reshape(experts * cap, columns)
    per_route = jnp.dot(pick, returned, preferred_element_type=F32).reshape(seqs, top, columns)
    combined = jnp.sum(per_route * route_weight[..., None], axis=1)
    layer_out = (own_resid + combined).astype(BF16)
    return (layer_out, new_state)


def solution(mesh):
    in_specs = (
        P("ep", None),
        P(),
        P(None, "tp"),
        P(None, "tp"),
        P(None, "tp"),
        P(None, "tp"),
        P(None, "tp"),
        P(None, "tp"),
        P("tp"),
        P("tp"),
        P("ep", "tp", None, None),
        P(),
        P("tp", None),
        P(),
        P("ep", None, "tp"),
        P("ep", None, "tp"),
        P("ep", "tp", None),
        P("ep", None),
        P("ep", None),
    )
    out_specs = (P("ep", "tp"), P("ep", "tp", None, None))
    return jax.shard_map(
        per_device, mesh=mesh, in_specs=in_specs, out_specs=out_specs, check_vma=False
    )
```

time: 116 us -> 66.3 us (0.57)
  waiting for transfers between devices: 36.2 us -> 2.95 us
  matrix products: 28 us -> 0.22 us
  Pallas kernels: 0 us -> 15.4 us
  between operations: 14.4 us -> 0.79 us
  blocking collectives: 19.1 us -> 31.7 us
  local copies, waits for them, and re-layouts: 2.86 us -> 11.8 us
  starting transfers between devices: 6.81 us -> 0.83 us
  other arithmetic: 7.91 us -> 2.04 us
    dot_general x14 -> x1, matrix products: 28 us -> 0.22 us  [per_device(): jnp.dot(pick, returned, preferred_element_type=F32)]
    psum x1 -> x0, waiting for transfers between devices: 20.1 us -> none  [per_device(): lax.psum(partial_value.astype(jnp.bfloat16), 'tp').astype(jnp.float32)]
    pallas_call x0 -> x3, Pallas kernels: none -> 15.4 us  [the longest x1 9.32 us: mixer(): pl.pallas_call(mixer_kernel, out_shape=(jax.ShapeDtypeStruct((seqs, wo.sh...]
    all_to_all x1 -> x2, blocking collectives: 16.9 us -> 31.7 us  [the longest x1 18.2 us: per_device(): lax.all_to_all(outgoing, 'ep', split_axis=0, concat_axis=0, tiled=True)]
    all_to_all x1 -> x0, waiting for transfers between devices: 10.2 us -> none  [per_device(): lax.all_to_all(summed, 'ep', split_axis=1, concat_axis=0, tiled=True)]
    unnamed x29 -> x33, local copies, waits for them, and re-layouts: 0.2 us -> 9.59 us
    all_to_all x1 -> x0, starting transfers between devices: 6.73 us -> none  [per_device(): lax.all_to_all(summed, 'ep', split_axis=1, concat_axis=0, tiled=True)]
    reduce_scatter x1 -> x0, waiting for transfers between devices: 5.89 us -> none  [per_device(): lax.psum_scatter(terms.astype(jnp.bfloat16), 'tp', scatter_dimension=3, t...]
  transfers between devices with their start and end apart: 3 -> 3, of which waited for: 3 -> 2; matrix products, arithmetic and copies ran while one was open for 1% -> 2% of each run, Pallas kernels for 0% -> 0%
where the time goes in v1:
time: 66.3 us; the launch traced here: 65.7 us
  blocking collectives  31.7 us (48%)
  Pallas kernels  15.4 us (23%)
  local copies, waits for them, and re-layouts  11.8 us (18%)
  waiting for transfers between devices  2.95 us (4%)
  other arithmetic  2.04 us (3%)
  starting transfers between devices  0.83 us (1%)
  between operations  0.79 us (1%)
    all_to_all x1, blocking collectives, per_device(): lax.all_to_all(outgoing, 'ep', split_axis=0, concat_axis=0, tiled=True)  18.2 us
    all_to_all x1, blocking collectives, per_device(): lax.all_to_all(summed, 'ep', split_axis=0, concat_axis=0, tiled=True)  13.5 us
    unnamed x33, local copies, waits for them, and re-layouts  9.59 us
    pallas_call x1, Pallas kernels, mixer(): pl.pallas_call(mixer_kernel, out_shape=(jax.ShapeDtypeStruct((seqs, wo.sh...  9.32 us
    pallas_call x1, Pallas kernels, expert(): pl.pallas_call(expert_kernel, out_shape=(half, half), in_specs=[pl.BlockS...  4.1 us
    pallas_call x1, Pallas kernels, dispatch(): pl.pallas_call(dispatch_kernel, out_shape=(jax.ShapeDtypeStruct((pick.sha...  2 us
    ppermute x1, waiting for transfers between devices, per_device(): lax.ppermute(send, 'tp', swap).astype(F32)  1.51 us
    ppermute x1, waiting for transfers between devices, per_device(): lax.ppermute(rows, 'tp', swap)  1.43 us
  transfers between devices with their start and end apart: 3, of which 2 were waited for; matrix products, arithmetic and copies ran while one was open for 2% of the time, Pallas kernels for 0%

profile of v1, /device:TPU:0, one launch (start us, length us, event | category | flops | bytes accessed | tf_op | source)
XLA Modules:
  0.0 65.7 jit_solution(15684839384440230734)
XLA Ops:
  0.6 1.6 %copy-done = bf16[2048,512]{1,0:T(8,128)(2,1)S(1)} copy-done((bf16[2048,512]{1,0:T(8,128)(2,1)S(1)}, bf16[2048,512]{1,0:T(8,128)(2,1)}, u32[]{:S(2)}) %copy-start) | copy-done | bytes 2097176
  2.2 1.6 %copy-done.1 = bf16[2048,512]{1,0:T(8,128)(2,1)S(1)} copy-done((bf16[2048,512]{1,0:T(8,128)(2,1)S(1)}, bf16[2048,512]{1,0:T(8,128)(2,1)}, u32[]{:S(2)}) %copy-start.1) | copy-done | bytes 2097176
  3.8 0.9 %copy-done.2 = bf16[24,2048]{1,0:T(8,128)(2,1)S(1)} copy-done((bf16[24,2048]{1,0:T(8,128)(2,1)S(1)}, bf16[24,2048]{1,0:T(8,128)(2,1)}, u32[]{:S(2)}) %copy-start.2) | copy-done | bytes 98328
  4.7 0.7 %copy-done.4 = bf16[2048,4]{0,1:T(4,128)(2,1)S(1)} copy-done((bf16[2048,4]{0,1:T(4,128)(2,1)S(1)}, bf16[2048,4]{0,1:T(4,128)(2,1)}, u32[]{:S(2)}) %copy-start.4) | copy-done | bytes 16408
  5.4 0.7 %copy-done.5 = bf16[2048,4]{0,1:T(4,128)(2,1)S(1)} copy-done((bf16[2048,4]{0,1:T(4,128)(2,1)S(1)}, bf16[2048,4]{0,1:T(4,128)(2,1)}, u32[]{:S(2)}) %copy-start.5) | copy-done | bytes 16408
  6.2 0.7 %copy-done.6 = f32[2048]{0:T(1024)S(1)} copy-done((f32[2048]{0:T(1024)S(1)}, f32[2048]{0:T(1024)}, u32[]{:S(2)}) %copy-start.6) | copy-done | bytes 8216
  6.8 0.7 copy-done.7
  7.5 0.7 copy-done.8
  8.2 0.7 copy-done.9
  8.8 9.3 %mixer.1 = (bf16[24,2048]{1,0:T(8,128)(2,1)S(1)}, f32[24,4,128,128]{3,2,1,0:T(8,128)}) custom-call(bf16[24,2048]{1,0:T(8,128)(2,1)S(1)} %copy-done.2, f32[1,2048]{1,0:T(1,128)S(1)} %bitcast.14, bf16[4,2048]{1,0:T(4,128)(2,1)S(1)} %bitcast.12, bf16[4,2048]{1,0:T(4,128)(2,1)S(1)} %bitcast.13, f32[1,4]{1,0:T(1,128)S(1)} %bitcast.15, f32[1,4]{1,0:T(1,128)S(1)} %bitcast.16, ...), custom_call_target="tpu_custom_call" | custom-call | tf_op jit(solution)/shard_map/mixer/pallas_call | solution.py:132
  18.2 0.6 collective-permute-start
  18.7 0.1 copy.35
  18.8 0.1 eq.57
  19.0 0.1 reduce_window_sum.11
  19.1 0.2 select_reduce_fusion
  19.2 0.1 reduce_sum.21
  19.3 0.1 copy.36
  19.4 0.1 fusion.2
  19.5 0.7 %copy.37.pick_ref = bf16[96,24]{1,0:T(8,128)(2,1)} copy(bf16[96,24]{0,1:T(8,128)(2,1)S(1)} %convert_element_type.20) | data formatting | bytes 9216 | tf_op jit(solution)/shard_map/convert_element_type | solution.py:269
  20.3 0.6 copy-done.13
  20.9 2.0 %dispatch.1 = (bf16[96,1024]{1,0:T(8,128)(2,1)}, f32[24,1024]{1,0:T(8,128)}) custom-call(s32[1]{0:T(128)} %bitcast.side_ref, bf16[24,2048]{1,0:T(8,128)(2,1)} %tokens_ref.3, bf16[24,2048]{1,0:T(8,128)(2,1)} %copy-done.3, bf16[24,2048]{1,0:T(8,128)(2,1)} %copy-done.13, f32[1,2048]{1,0:T(1,128)} %bitcast.18, bf16[96,24]{1,0:T(8,128)(2,1)} %copy.37.pick_ref), custom_call_target="tpu_custom_call" | custom-call | tf_op jit(solution)/shard_map/dispatch/pallas_call | solution.py:174
  22.9 1.0 %reshape.62 = bf16[16,6,1024]{2,1,0:T(8,128)(2,1)S(1)} reshape(bf16[96,1024]{1,0:T(8,128)(2,1)} %get-tuple-element.10) | data formatting | bytes 393216 | tf_op jit(solution)/shard_map/reshape | solution.py:272
  23.9 18.2 %all_to_all.10 = bf16[16,6,1024]{2,1,0:T(8,128)(2,1)S(1)} all-to-all(bf16[16,6,1024]{2,1,0:T(8,128)(2,1)S(1)} %reshape.62), channel_id=1, replica_groups=mesh['ep'=16,'tp'=2] {'ep'}, dimensions={0} | all-to-all | bytes 393216 | tf_op jit(solution)/shard_map/all_to_all | solution.py:273
  42.3 1.4 %collective-permute-done.1.oth_ref = bf16[96,1024]{1,0:T(8,128)(2,1)S(1)} collective-permute-done((bf16[96,1024]{1,0:T(8,128)(2,1)S(1)}, bf16[96,1024]{1,0:T(8,128)(2,1)S(1)}, u32[]{:S(2)}, u32[]{:S(2)}) %collective-permute-start.1) | collective-permute-done | bytes 196640 | tf_op jit(solution)/shard_map/ppermute | solution.py:275
  43.7 0.7 %copy-done.11 = bf16[96,1024]{1,0:T(8,128)(2,1)} copy-done((bf16[96,1024]{1,0:T(8,128)(2,1)}, bf16[96,1024]{1,0:T(8,128)(2,1)S(1)}, u32[]{:S(2)}) %copy-start.11) | copy-done | bytes 196632
  44.4 4.1 %expert.1 = (bf16[96,1024]{1,0:T(8,128)(2,1)}, bf16[96,1024]{1,0:T(8,128)(2,1)}) custom-call(s32[1]{0:T(128)} %bitcast.side_ref, bf16[96,1024]{1,0:T(8,128)(2,1)} %copy-done.10, bf16[96,1024]{1,0:T(8,128)(2,1)} %copy-done.11, bf16[1,2048,256]{2,1,0:T(8,128)(2,1)} %wg_hbm.1, bf16[1,2048,256]{2,1,0:T(8,128)(2,1)} %wu_hbm.1, bf16[1,256,2048]{2,1,0:T(8,128)(2,1)} %wd_hbm.1), custom_call_target="tpu_custom_call" | custom-call | tf_op jit(solution)/shard_map/expert/pallas_call | solution.py:217
  48.5 0.2 collective-permute-start.2
  48.7 1.5 %collective-permute-done.2 = bf16[96,1024]{1,0:T(8,128)(2,1)S(1)} collective-permute-done((bf16[96,1024]{1,0:T(8,128)(2,1)}, bf16[96,1024]{1,0:T(8,128)(2,1)S(1)}, u32[]{:S(2)}, u32[]{:S(2)}) %collective-permute-start.2) | collective-permute-done | bytes 196640 | tf_op jit(solution)/shard_map/ppermute | solution.py:276
  50.2 1.0 %add_convert_fusion = bf16[96,1024]{1,0:T(8,128)(2,1)S(1)} fusion(bf16[96,1024]{1,0:T(8,128)(2,1)S(1)} %collective-permute-done.2, bf16[96,1024]{1,0:T(8,128)(2,1)} %get-tuple-element.11), kind=kLoop, calls=%fused_computation.2 | loop fusion | flops 393216 | bytes 589824 | tf_op jit(solution)/shard_map/convert_element_type | solution.py:276
  51.3 13.5 %all_to_all.11 = bf16[16,6,1024]{2,1,0:T(8,128)(2,1)S(1)} all-to-all(bf16[16,6,1024]{2,1,0:T(8,128)(2,1)S(1)} %reshape.64), channel_id=1, replica_groups=mesh['ep'=16,'tp'=2] {'ep'}, dimensions={0} | all-to-all | bytes 393216 | tf_op jit(solution)/shard_map/all_to_all | solution.py:278
  64.9 0.2 fusion
  65.1 0.6 add_convert_fusion.1
  (29 shorter events, 0.4 us)
Async XLA Ops:
  0.6 1.6 %copy-start = (bf16[2048,512]{1,0:T(8,128)(2,1)S(1)}, bf16[2048,512]{1,0:T(8,128)(2,1)}, u32[]{:S(2)}) copy-start(bf16[2048,512]{1,0:T(8,128)(2,1)} %wq_hbm.1) | copy-start | bytes 6291460
  2.2 1.6 %copy-start.1 = (bf16[2048,512]{1,0:T(8,128)(2,1)S(1)}, bf16[2048,512]{1,0:T(8,128)(2,1)}, u32[]{:S(2)}) copy-start(bf16[2048,512]{1,0:T(8,128)(2,1)} %wk_hbm.1) | copy-start | bytes 6291460
  3.8 0.9 %copy-start.2 = (bf16[24,2048]{1,0:T(8,128)(2,1)S(1)}, bf16[24,2048]{1,0:T(8,128)(2,1)}, u32[]{:S(2)}) copy-start(bf16[24,2048]{1,0:T(8,128)(2,1)} %tokens_ref.3) | copy-start | bytes 294916
  4.7 0.7 %copy-start.4 = (bf16[2048,4]{0,1:T(4,128)(2,1)S(1)}, bf16[2048,4]{0,1:T(4,128)(2,1)}, u32[]{:S(2)}) copy-start(bf16[2048,4]{0,1:T(4,128)(2,1)} %param.25) | copy-start | bytes 49156
  5.4 0.7 %copy-start.5 = (bf16[2048,4]{0,1:T(4,128)(2,1)S(1)}, bf16[2048,4]{0,1:T(4,128)(2,1)}, u32[]{:S(2)}) copy-start(bf16[2048,4]{0,1:T(4,128)(2,1)} %param.26) | copy-start | bytes 49156
  6.1 0.7 %copy-start.6 = (f32[2048]{0:T(1024)S(1)}, f32[2048]{0:T(1024)}, u32[]{:S(2)}) copy-start(f32[2048]{0:T(1024)} %param.20) | copy-start | bytes 24580
  6.8 0.7 copy-start.7
  7.5 0.7 copy-start.8
  8.2 0.7 copy-start.9
  8.8 9.9 %copy-start.14 = (s32[24,2]{0,1:T(2,128)S(1)}, s32[24,2]{0,1:T(2,128)}, u32[]{:S(2)}) copy-start(s32[24,2]{0,1:T(2,128)} %param.36) | copy-start | bytes 580
  18.1 2.1 %copy-start.3 = (bf16[24,2048]{1,0:T(8,128)(2,1)}, bf16[24,2048]{1,0:T(8,128)(2,1)S(1)}, u32[]{:S(2)}) copy-start(bf16[24,2048]{1,0:T(8,128)(2,1)S(1)} %get-tuple-element.8.part_ref) | copy-start | bytes 294916
  18.2 2.1 %collective-permute-start = (bf16[24,2048]{1,0:T(8,128)(2,1)S(1)}, bf16[24,2048]{1,0:T(8,128)(2,1)S(1)}, u32[]{:S(2)}, u32[]{:S(2)}) collective-permute-start(bf16[24,2048]{1,0:T(8,128)(2,1)S(1)} %get-tuple-element.8.part_ref), channel_id=1, source_target_pairs={{0,1},{1,0},{2,3},{3,2},{4,5},{5,4},{6,7},{7,6},{8,9},{9,8},{10,11... | collective-permute-start | bytes 294920 | tf_op jit(solution)/shard_map/ppermute | solution.py:260
  20.2 0.6 copy-start.13
  42.2 1.5 %copy-start.10 = (bf16[96,1024]{1,0:T(8,128)(2,1)}, bf16[96,1024]{1,0:T(8,128)(2,1)S(1)}, u32[]{:S(2)}) copy-start(bf16[96,1024]{1,0:T(8,128)(2,1)S(1)} %reshape.63.own_ref) | copy-start | bytes 589828
  42.2 22.7 %copy-start.15 = (f32[24,2]{0,1:T(2,128)S(1)}, f32[24,2]{0,1:T(2,128)}, u32[]{:S(2)}) copy-start(f32[24,2]{0,1:T(2,128)} %param.37) | copy-start | bytes 580
  42.2 22.9 %copy-start.12 = (f32[24,1024]{1,0:T(8,128)S(1)}, f32[24,1024]{1,0:T(8,128)}, u32[]{:S(2)}) copy-start(f32[24,1024]{1,0:T(8,128)} %get-tuple-element.9) | copy-start | bytes 294916
  42.2 1.5 %collective-permute-start.1 = (bf16[96,1024]{1,0:T(8,128)(2,1)S(1)}, bf16[96,1024]{1,0:T(8,128)(2,1)S(1)}, u32[]{:S(2)}, u32[]{:S(2)}) collective-permute-start(bf16[96,1024]{1,0:T(8,128)(2,1)S(1)} %reshape.63.own_ref), channel_id=1, source_target_pairs={{0,1},{1,0},{2,3},{3,2},{4,5},{5,4},{6,7},{7,6},{8,9},{9,8},{10,11... | collective-permute-start | bytes 589832 | tf_op jit(solution)/shard_map/ppermute | solution.py:275
  43.7 0.7 %copy-start.11 = (bf16[96,1024]{1,0:T(8,128)(2,1)}, bf16[96,1024]{1,0:T(8,128)(2,1)S(1)}, u32[]{:S(2)}) copy-start(bf16[96,1024]{1,0:T(8,128)(2,1)S(1)} %collective-permute-done.1.oth_ref) | copy-start | bytes 589828
  48.5 1.7 %collective-permute-start.2 = (bf16[96,1024]{1,0:T(8,128)(2,1)}, bf16[96,1024]{1,0:T(8,128)(2,1)S(1)}, u32[]{:S(2)}, u32[]{:S(2)}) collective-permute-start(bf16[96,1024]{1,0:T(8,128)(2,1)} %get-tuple-element.12), channel_id=1, source_target_pairs={{0,1},{1,0},{2,3},{3,2},{4,5},{5,4},{6,7},{7,6},{8,9},{9,8},{10,11... | collective-permute-start | bytes 589832 | tf_op jit(solution)/shard_map/ppermute | solution.py:276
